TPU v7x, 256 devices: a whole 4x4x8 slice. The times are simulated.
256 devices in a mesh: sp: 16 (over y, x), tp: 16 (over z, core).
Axes of the slice: x: 4, y: 4, z: 8, core: 2. Of those that a mesh axis runs over, the one named last changes fastest.
Arguments:
- conv_value: bfloat16 [1024, 16384], P('tp', 'sp'), may hold values from -6 to 6
- conv_gate: bfloat16 [1024, 16384], P('tp', 'sp'), may hold values from -6 to 6
- conv_taps: float32 [1024, 31], P('tp'), may hold values from -2.2 to 2.2
- norm_gain: float32 [1024], replicated, may hold values from 0.1 to 1.9
- norm_bias: float32 [1024], replicated, may hold values from -3 to 3
- out_weight: bfloat16 [1024, 2048], replicated, may hold values from -0.1875 to 0.1875
- stream: bfloat16 [16384, 2048], P(('sp', 'tp')), may hold values from -6 to 6
- routes: int32 [16384, 2], P(('sp', 'tp')), may hold values from 0 to 15, all different within a row; in each aligned block of 64 rows (0 to 63, 64 to 127, ...) at most 8 rows name the same one
- route_weights: float32 [16384, 2], P(('sp', 'tp')), may hold values from 0.2 to 1
- expert_gain: float32 [2048], replicated, may hold values from 0.1 to 1.9
- expert_gate: bfloat16 [16, 2048, 7168], P('sp', None, 'tp'), may hold values from -0.125 to 0.125
- expert_up: bfloat16 [16, 2048, 7168], P('sp', None, 'tp'), may hold values from -0.125 to 0.125
- expert_down: bfloat16 [16, 7168, 2048], P('sp', 'tp'), may hold values from -0.0625 to 0.0625
Outputs:
- mixed: bfloat16 [16384, 2048], P(('sp', 'tp'))
Inputs may be any that keep to these rules, and one draw needn't show every extreme that they name: `routes`: within each device's 64 rows every expert is named exactly 8 times; a row names distinct experts.
All inputs are finite; a program needn't handle non-finite values.
Results may differ from a plain program's by a relative error of at most 0.014.
Values may be sent and summed in bfloat16 or wider, within the bound.
A program may use at most 64 MiB of HBM per device.

v0:
```python
import jax
import jax.numpy as jnp
from jax import lax
from jax.sharding import PartitionSpec as P

epsilon = 1e-06


def shifted(value, axis, steps):
    count = lax.axis_size(axis)
    initial, last = (max(0, -steps), min(count, count - steps))
    return lax.ppermute(value, axis, [(source, source + steps) for source in range(initial, last)])


def per_device(
    conv_value,
    conv_gate,
    conv_taps,
    norm_gain,
    norm_bias,
    out_weight,
    stream,
    routes,
    route_weights,
    expert_gain,
    expert_gate,
    expert_up,
    expert_down,
):
    f32 = jnp.float32
    local_ch = conv_value.shape[0]
    run_len = conv_value.shape[1]
    kernel_len = conv_taps.shape[1]
    gated_input = (conv_value.astype(f32) * jax.nn.sigmoid(conv_gate.astype(f32))).astype(
        jnp.bfloat16
    )
    left_rim = shifted(gated_input[:, run_len - (kernel_len - 1) :], "sp", 1)
    padded = jnp.concatenate([left_rim, gated_input], axis=1).astype(f32)
    conv_sum = jnp.zeros((local_ch, run_len), f32)
    for offset in range(kernel_len):
        conv_sum = (
            conv_sum + conv_taps[:, offset : offset + 1] * padded[:, offset : offset + run_len]
        )
    conv_out = conv_sum.astype(jnp.bfloat16)
    whole_conv = lax.all_to_all(conv_out, "tp", split_axis=1, concat_axis=0, tiled=True).astype(f32)
    center = jnp.mean(whole_conv, axis=0, keepdims=True)
    spread = jnp.mean((whole_conv - center) ** 2, axis=0, keepdims=True)
    scaled = (whole_conv - center) * lax.rsqrt(spread + epsilon) * norm_gain[:, None] + norm_bias[
        :, None
    ]
    token_major = jax.nn.silu(scaled).astype(jnp.bfloat16)
    projected = lax.dot_general(
        token_major, out_weight, (((0,), (0,)), ((), ())), preferred_element_type=f32
    )
    residual = (stream.astype(f32) + projected).astype(jnp.bfloat16)
    res_float = residual.astype(f32)
    normed = (
        res_float
        * lax.rsqrt(jnp.mean(res_float * res_float, axis=1, keepdims=True) + epsilon)
        * expert_gain
    ).astype(jnp.bfloat16)
    tok_rows = stream.shape[0]
    width = stream.shape[1]
    top_count = routes.shape[1]
    experts = lax.axis_size("sp")
    capacity = top_count * tok_rows // experts
    flat_ids = routes.reshape(-1)
    onehot = (flat_ids[:, None] == jnp.arange(experts, dtype=jnp.int32)[None, :]).astype(jnp.int32)
    before = jnp.cumsum(onehot, axis=0) - onehot
    rank = jnp.sum(before * onehot, axis=1)
    slots = flat_ids * capacity + rank
    chooser = jnp.any(
        slots.reshape(tok_rows, top_count)[None, :, :]
        == jnp.arange(experts * capacity, dtype=jnp.int32)[:, None, None],
        axis=2,
    ).astype(jnp.bfloat16)
    send_rows = (
        jnp.dot(chooser, normed, preferred_element_type=f32)
        .astype(jnp.bfloat16)
        .reshape(experts, capacity, width)
    )
    gate_w = expert_gate[0]
    up_w = expert_up[0]
    down_w = expert_down[0]
    received = lax.all_to_all(send_rows, "sp", split_axis=0, concat_axis=0, tiled=True)
    flat_recv = received.reshape(-1, width)
    piece = lax.all_gather(flat_recv, "tp", axis=0, tiled=True)
    gate_val = jnp.dot(piece, gate_w, preferred_element_type=f32)
    up_val = jnp.dot(piece, up_w, preferred_element_type=f32)
    hidden = (jax.nn.silu(gate_val) * up_val).astype(jnp.bfloat16)
    summed = lax.psum_scatter(
        jnp.dot(hidden, down_w, preferred_element_type=f32).astype(jnp.bfloat16),
        "tp",
        scatter_dimension=0,
        tiled=True,
    )
    result = summed.reshape(received.shape)
    returned = lax.all_to_all(result, "sp", split_axis=0, concat_axis=0, tiled=True)
    picked = returned.reshape(experts * capacity, width)[slots].reshape(tok_rows, top_count, width)
    expert_sum = jnp.sum(picked.astype(f32) * route_weights[:, :, None], axis=1)
    return (res_float + expert_sum).astype(jnp.bfloat16)


def solution(mesh):
    return jax.shard_map(
        per_device,
        mesh=mesh,
        in_specs=(
            P("tp", "sp"),
            P("tp", "sp"),
            P("tp", None),
            P(),
            P(),
            P(),
            P(("sp", "tp"), None),
            P(("sp", "tp"), None),
            P(("sp", "tp"), None),
            P(),
            P("sp", None, "tp"),
            P("sp", None, "tp"),
            P("sp", "tp", None),
        ),
        out_specs=P(("sp", "tp"), None),
        check_vma=False,
    )
```

profile of v0, /device:TPU:2, one launch (start us, length us, event | category | flops | bytes accessed | tf_op | source)
XLA Modules:
  0.0 225.3 jit_solution(4182957621673231946)
XLA Ops:
  6.5 0.0 copy-start
  6.5 1.2 multiply_convert_fusion.4
  7.7 0.1 slice.254
  7.8 3.4 %collective-permute-start = (bf16[64,30]{1,0:T(8,128)(2,1)S(1)}, bf16[64,30]{1,0:T(8,128)(2,1)S(1)}, u32[]{:S(2)}, u32[]{:S(2)}) collective-permute-start(bf16[64,30]{1,0:T(8,128)(2,1)S(1)} %slice.254), channel_id=1, source_target_pairs={{0,16},{16,32},{32,48},{48,64},{64,80},{80,96},{96,112},{112,128},... | collective-permute-start | bytes 11528 | tf_op jit(solution)/shard_map/ppermute | solution.py:12
  11.2 1.0 slice_bitcast_fusion.30
  12.2 1.0 slice_bitcast_fusion.29
  13.2 0.8 copy.28
  14.0 0.1 eq.28
  14.1 0.1 fusion.47
  14.2 0.2 reduce_window_sum.11
  14.4 0.2 select_reduce_fusion
  14.6 0.1 reduce_sum.52
  14.7 0.0 collective-permute-done
  14.7 0.1 maximum_convert_fusion
  14.8 2.7 %fusion.10 = bf16[64,1024]{1,0:T(8,128)(2,1)S(1)} fusion(f32[64,1054]{1,0:T(8,128)S(1)} %maximum_convert_fusion, f32[64]{0:T(128)S(1)} %get-tuple-element.36, f32[64]{0:T(128)S(1)} %get-tuple-element.37, f32[64]{0:T(128)S(1)} %get-tuple-element.8, f32[64]{0:T(128)S(1)} %get-tuple-element.9, f32[64]{0:T(128)S(1)} %get-tuple-element.10, ...), kind=kLoop, calls=%fused_computation.23 | loop fusion | flops 4063232 | bytes 8265472 | tf_op jit(solution)/shard_map/convert_element_type | solution.py:44
  17.5 0.0 copy-start.1
  17.5 0.0 copy-start.3
  17.5 0.0 copy-start.4
  17.5 0.2 copy.26
  17.7 0.9 reshape.99
  18.6 8.6 %all-to-all-start = ((bf16[16,2,2048]{2,1,0:T(2,128)(2,1)}), bf16[16,2,2048]{2,1,0:T(2,128)(2,1)S(1)}, u32[]{:S(2)}, u32[]{:S(2)}) async-start(bf16[16,2,2048]{2,1,0:T(2,128)(2,1)} %reshape.99), calls=%async_computation | async-start | bytes 262144 | tf_op jit(solution)/shard_map/all_to_all | solution.py:45
  27.2 0.0 all-gather.2.cloned.1.call-start
  27.3 0.1 copy.30
  27.3 0.1 fusion.48
  27.4 8.4 %all-to-all-done = bf16[16,2,2048]{2,1,0:T(2,128)(2,1)S(1)} async-done(((bf16[16,2,2048]{2,1,0:T(2,128)(2,1)}), bf16[16,2,2048]{2,1,0:T(2,128)(2,1)S(1)}, u32[]{:S(2)}, u32[]{:S(2)}) %all-to-all-start) | async-done | bytes 131104 | tf_op jit(solution)/shard_map/all_to_all | solution.py:45
  35.8 0.2 reshape.100
  36.1 0.2 convert_reduce_fusion
  36.3 0.0 copy-start.2
  36.3 0.3 copy.27
  36.6 0.2 reshape.89
  36.8 0.3 fusion.8
  37.0 0.0 copy-done.1
  37.0 0.0 copy-done.3
  37.0 0.0 copy-done.4
  37.1 3.3 %multiply_reduce_fusion.1 = (f32[64]{0:T(128)S(1)}, f32[64,2048]{1,0:T(8,128)S(1)}) fusion(bf16[1024,2048]{1,0:T(8,128)(2,1)} %param.18, f32[1024,64]{0,1:T(8,128)S(1)} %reshape.89, f32[1024]{0:T(1024)S(1)} %copy-done.3, f32[1024]{0:T(1024)S(1)} %copy-done.4, f32[64]{0:T(128)S(1)} %add_rsqrt_fusion.1, f32[64]{0:T(128)S(1)} %broadcast_multiply_fusion.1, ...), kind=kOutput, calls=%fused_computation.20 | convolution fusion | flops 269811648 | bytes 5251840 | tf_op jit(solution)/shard_map/dot_general | solution.py:52
  40.4 0.0 copy-done.2
  40.4 0.4 fusion
  40.7 18.1 %all_to_all.23 = bf16[16,8,2048]{2,1,0:T(8,128)(2,1)} all-to-all(bf16[16,8,2048]{2,1,0:T(8,128)(2,1)S(1)} %fusion), channel_id=1, replica_groups=mesh['sp'=16,'tp'=16] {'sp'}, dimensions={0} | all-to-all | bytes 1048576 | tf_op jit(solution)/shard_map/all_to_all | solution.py:85
  58.8 0.0 all-gather.2.cloned.1.call-update
  58.8 0.2 reduce-scatter.2.cloned.1.call-start
  59.1 49.8 %all-gather.2.cloned.1.call-done = bf16[2048,2048]{1,0:T(8,128)(2,1)} async-done(((bf16[128,2048]{1,0:T(8,128)(2,1)}), bf16[2048,2048]{1,0:T(8,128)(2,1)}) %all-gather.2.cloned.1.call-update) | async-done | bytes 8388624 | tf_op jit(solution)/shard_map/all_gather | solution.py:87
  108.8 0.0 copy-start.6
  108.8 0.0 copy-start.7
  108.8 7.2 %fusion.5 = f32[2048,448]{0,1:T(8,128)S(1)} fusion(bf16[2048,2048]{1,0:T(8,128)(2,1)} %all-gather.2.cloned.1.call-done, bf16[1,2048,448]{1,2,0:T(8,128)(2,1)} %param.23), kind=kOutput, calls=%fused_computation.10 | convolution fusion | flops 3758096384 | bytes 13893632 | tf_op jit(solution)/shard_map/dot_general | solution.py:88
  116.0 0.0 copy-done.6
  116.0 0.0 copy-done.7
  116.0 4.3 %multiply_convert_fusion = bf16[2048,448]{0,1:T(8,128)(2,1)S(1)} fusion(f32[2048,448]{0,1:T(8,128)S(1)} %fusion.5, bf16[2048,2048]{1,0:T(8,128)(2,1)S(1)} %copy-done.6, bf16[1,2048,448]{1,2,0:T(8,128)(2,1)S(1)} %copy-done.7), kind=kOutput, calls=%fused_computation.2 | convolution fusion | flops 3763601408 | bytes 15728640 | tf_op jit(solution)/shard_map/dot_general | solution.py:89
  120.3 0.0 copy-done
  120.3 6.9 %convolution_convert_fusion = bf16[2048,2048]{1,0:T(8,128)(2,1)} fusion(bf16[2048,448]{0,1:T(8,128)(2,1)S(1)} %multiply_convert_fusion, bf16[1,448,2048]{2,1,0:T(8,128)(2,1)S(1)} %copy-done), kind=kOutput, calls=%fused_computation.1 | convolution fusion | flops 3762290688 | bytes 12058624 | tf_op jit(solution)/shard_map/dot_general | solution.py:92
  127.2 0.0 copy-start.5
  127.2 0.0 reduce-scatter.2.cloned.1.call-update
  127.2 69.5 %reduce-scatter.2.cloned.1.call-done = bf16[128,2048]{1,0:T(8,128)(2,1)} async-done(((bf16[2048,2048]{1,0:T(8,128)(2,1)}), bf16[128,2048]{1,0:T(8,128)(2,1)}) %reduce-scatter.2.cloned.1.call-update) | async-done | bytes 524304 | tf_op jit(solution)/shard_map/reduce_scatter | solution.py:91
  196.8 7.1 %all-to-all-start.2 = ((bf16[16,8,2048]{2,1,0:T(8,128)(2,1)}), bf16[16,8,2048]{2,1,0:T(8,128)(2,1)S(1)}, u32[]{:S(2)}, u32[]{:S(2)}) async-start(bf16[16,8,2048]{2,1,0:T(8,128)(2,1)} %bitcast.100), calls=%async_computation.3 | async-start | bytes 1048576 | tf_op jit(solution)/shard_map/all_to_all | solution.py:98
  203.9 0.1 mul.497
  204.0 0.0 copy-done.5
  204.0 0.1 copy.31
  204.2 8.5 %all-to-all-done.2 = bf16[16,8,2048]{2,1,0:T(8,128)(2,1)S(1)} async-done(((bf16[16,8,2048]{2,1,0:T(8,128)(2,1)}), bf16[16,8,2048]{2,1,0:T(8,128)(2,1)S(1)}, u32[]{:S(2)}, u32[]{:S(2)}) %all-to-all-start.2) | async-done | bytes 524320 | tf_op jit(solution)/shard_map/all_to_all | solution.py:98
  212.7 1.7 gather_fusion
  214.4 1.7 reshape.90
  216.1 1.6 multiply_reduce_fusion
  217.7 0.8 add_convert_fusion
  (7 shorter events, 0.1 us)
Async XLA Ops:
  6.5 113.8 %copy-start = (bf16[1,448,2048]{2,1,0:T(8,128)(2,1)S(1)}, bf16[1,448,2048]{2,1,0:T(8,128)(2,1)}, u32[]{:S(2)}) copy-start(bf16[1,448,2048]{2,1,0:T(8,128)(2,1)} %param.25) | copy-start | bytes 5505028
  7.8 6.9 %collective-permute-start = (bf16[64,30]{1,0:T(8,128)(2,1)S(1)}, bf16[64,30]{1,0:T(8,128)(2,1)S(1)}, u32[]{:S(2)}, u32[]{:S(2)}) collective-permute-start(bf16[64,30]{1,0:T(8,128)(2,1)S(1)} %slice.254), channel_id=1, source_target_pairs={{0,16},{16,32},{32,48},{48,64},{64,80},{80,96},{96,112},{112,128},... | collective-permute-start | bytes 11528 | tf_op jit(solution)/shard_map/ppermute | solution.py:12
  17.5 19.5 %copy-start.1 = (bf16[64,2048]{1,0:T(8,128)(2,1)S(1)}, bf16[64,2048]{1,0:T(8,128)(2,1)}, u32[]{:S(2)}) copy-start(bf16[64,2048]{1,0:T(8,128)(2,1)} %param.19) | copy-start | bytes 786436
  17.5 19.5 %copy-start.3 = (f32[1024]{0:T(1024)S(1)}, f32[1024]{0:T(1024)}, u32[]{:S(2)}) copy-start(f32[1024]{0:T(1024)} %param.17) | copy-start | bytes 12292
  17.5 19.5 %copy-start.4 = (f32[1024]{0:T(1024)S(1)}, f32[1024]{0:T(1024)}, u32[]{:S(2)}) copy-start(f32[1024]{0:T(1024)} %param.16) | copy-start | bytes 12292
  18.6 17.2 %all-to-all-start = ((bf16[16,2,2048]{2,1,0:T(2,128)(2,1)}), bf16[16,2,2048]{2,1,0:T(2,128)(2,1)S(1)}, u32[]{:S(2)}, u32[]{:S(2)}) async-start(bf16[16,2,2048]{2,1,0:T(2,128)(2,1)} %reshape.99), calls=%async_computation | async-start | bytes 262144 | tf_op jit(solution)/shard_map/all_to_all | solution.py:45
  27.2 81.6 %all-gather.2.cloned.1.call-start = ((), (), s32[]{:S(2)}) async-start(), calls=%async_computation.4 | async-start | bytes 8912896 | tf_op jit(solution)/shard_map/all_gather | solution.py:87
  36.3 4.1 %copy-start.2 = (f32[2048]{0:T(1024)S(1)}, f32[2048]{0:T(1024)}, u32[]{:S(2)}) copy-start(f32[2048]{0:T(1024)} %param.22) | copy-start | bytes 24580
  58.8 138.0 %reduce-scatter.2.cloned.1.call-start = ((), (), s32[]{:S(2)}) async-start(), calls=%async_computation.5 | async-start | bytes 8912896 | tf_op jit(solution)/shard_map/reduce_scatter | solution.py:91
  108.8 7.2 %copy-start.6 = (bf16[2048,2048]{1,0:T(8,128)(2,1)S(1)}, bf16[2048,2048]{1,0:T(8,128)(2,1)}, u32[]{:S(2)}) copy-start(bf16[2048,2048]{1,0:T(8,128)(2,1)} %all-gather.2.cloned.1.call-done) | copy-start | bytes 25165828
  108.8 7.2 %copy-start.7 = (bf16[1,2048,448]{1,2,0:T(8,128)(2,1)S(1)}, bf16[1,2048,448]{1,2,0:T(8,128)(2,1)}, u32[]{:S(2)}) copy-start(bf16[1,2048,448]{1,2,0:T(8,128)(2,1)} %param.24) | copy-start | bytes 5505028
  127.2 76.8 %copy-start.5 = (f32[64,2]{0,1:T(2,128)S(1)}, f32[64,2]{0,1:T(2,128)}, u32[]{:S(2)}) copy-start(f32[64,2]{0,1:T(2,128)} %param.21) | copy-start | bytes 1540
  196.8 15.9 %all-to-all-start.2 = ((bf16[16,8,2048]{2,1,0:T(8,128)(2,1)}), bf16[16,8,2048]{2,1,0:T(8,128)(2,1)S(1)}, u32[]{:S(2)}, u32[]{:S(2)}) async-start(bf16[16,8,2048]{2,1,0:T(8,128)(2,1)} %bitcast.100), calls=%async_computation.3 | async-start | bytes 1048576 | tf_op jit(solution)/shard_map/all_to_all | solution.py:98
Sparse Core Ops, SparseCore 0:
  59.0 49.8 all-gather.1
  127.4 69.3 reduce-scatter.1
where the time goes:
time: 226 us; the launch traced here: 225 us
  waiting for transfers between devices  136 us (60%)
  matrix products  22 us (10%)
  starting transfers between devices  19.3 us (9%)
  blocking collectives  18.1 us (8%)
  between operations  13.7 us (6%)
  local copies, waits for them, and re-layouts  8.64 us (4%)
  other arithmetic  7.29 us (3%)
    reduce_scatter x1, waiting for transfers between devices, per_device(): lax.psum_scatter(jnp.dot(hidden, down_w, preferred_element_type=f32).asty...  69.5 us
    all_gather x1, waiting for transfers between devices, per_device(): piece = lax.all_gather(flat_recv, 'tp', axis=0, tiled=True)  49.8 us
    all_to_all x1, blocking collectives, per_device(): lax.all_to_all(send_rows, 'sp', split_axis=0, concat_axis=0, tiled=True)  18.1 us
    all_to_all x1, starting transfers between devices, per_device(): lax.all_to_all(conv_out, 'tp', split_axis=1, concat_axis=0, tiled=True)  8.57 us
    all_to_all x1, waiting for transfers between devices, per_device(): lax.all_to_all(result, 'sp', split_axis=0, concat_axis=0, tiled=True)  8.52 us
    all_to_all x1, waiting for transfers between devices, per_device(): lax.all_to_all(conv_out, 'tp', split_axis=1, concat_axis=0, tiled=True)  8.41 us
    dot_general x1, matrix products, per_device(): gate_val = jnp.dot(piece, gate_w, preferred_element_type=f32)  7.17 us
    all_to_all x1, starting transfers between devices, per_device(): lax.all_to_all(result, 'sp', split_axis=0, concat_axis=0, tiled=True)  7.1 us
  transfers between devices with their start and end apart: 5, of which 4 were waited for; matrix products, arithmetic and copies ran while one was open for 2% of the time, Pallas kernels for 0%

commit v1 on v0

--- a/solution.py
+++ b/solution.py
@@ -84,7 +84,9 @@
     down_w = expert_down[0]
     received = lax.all_to_all(send_rows, "sp", split_axis=0, concat_axis=0, tiled=True)
     flat_recv = received.reshape(-1, width)
-    piece = lax.all_gather(flat_recv, "tp", axis=0, tiled=True)
+    piece = jnp.concatenate(
+        lax.all_to_all(jnp.stack([flat_recv] * lax.psum(1, "tp"), 0), "tp", 0, 0), 0
+    )
     gate_val = jnp.dot(piece, gate_w, preferred_element_type=f32)
     up_val = jnp.dot(piece, up_w, preferred_element_type=f32)
     hidden = (jax.nn.silu(gate_val) * up_val).astype(jnp.bfloat16)

time: 226 us -> 358 us (1.58)
  blocking collectives: 18.1 us -> 205 us
  waiting for transfers between devices: 136 us -> 83.6 us
    all_to_all x0 -> x1, blocking collectives: none -> 187 us  [per_device(): lax.all_to_all(jnp.stack([flat_recv] * lax.psum(1, 'tp'), 0), 'tp', 0, 0)]
    all_gather x1 -> x0, waiting for transfers between devices: 49.8 us -> none  [per_device(): piece = lax.all_gather(flat_recv, 'tp', axis=0, tiled=True)]
  transfers between devices with their start and end apart: 5 -> 4, of which waited for: 4 -> 3; matrix products, arithmetic and copies ran while one was open for 2% -> 1% of each run, Pallas kernels for 0% -> 0%
where the time goes in v1:
time: 358 us; the launch traced here: 357 us
  blocking collectives  205 us (57%)
  waiting for transfers between devices  83.6 us (23%)
  starting transfers between devices  19.1 us (5%)
  matrix products  18.8 us (5%)
  between operations  13.7 us (4%)
  local copies, waits for them, and re-layouts  9.7 us (3%)
  other arithmetic  7.27 us (2%)
    all_to_all x1, blocking collectives, per_device(): lax.all_to_all(jnp.stack([flat_recv] * lax.psum(1, 'tp'), 0), 'tp', 0, 0)  187 us
    reduce_scatter x1, waiting for transfers between devices, per_device(): lax.psum_scatter(jnp.dot(hidden, down_w, preferred_element_type=f32).asty...  66.7 us
    all_to_all x1, blocking collectives, per_device(): lax.all_to_all(send_rows, 'sp', split_axis=0, concat_axis=0, tiled=True)  18 us
    all_to_all x1, starting transfers between devices, per_device(): lax.all_to_all(conv_out, 'tp', split_axis=1, concat_axis=0, tiled=True)  8.57 us
    all_to_all x1, waiting for transfers between devices, per_device(): lax.all_to_all(result, 'sp', split_axis=0, concat_axis=0, tiled=True)  8.52 us
    all_to_all x1, waiting for transfers between devices, per_device(): lax.all_to_all(conv_out, 'tp', split_axis=1, concat_axis=0, tiled=True)  8.41 us
  transfers between devices with their start and end apart: 4, of which 3 were waited for; matrix products, arithmetic and copies ran while one was open for 1% of the time, Pallas kernels for 0%

profile of v1, /device:TPU:2, one launch (start us, length us, event | category | flops | bytes accessed | tf_op | source)
XLA Modules:
  0.0 357.4 jit_solution(16689211710930129502)
XLA Ops:
  6.5 0.0 copy-start
  6.5 1.2 multiply_convert_fusion.4
  7.7 0.1 slice.254
  7.8 3.4 collective-permute-start
  11.2 1.0 slice_bitcast_fusion.30
  12.2 1.0 slice_bitcast_fusion.29
  13.2 0.8 copy.28
  14.0 0.1 eq.28
  14.1 0.1 fusion.47
  14.2 0.2 reduce_window_sum.11
  14.4 0.2 select_reduce_fusion
  14.6 0.1 reduce_sum.52
  14.7 0.0 collective-permute-done
  14.7 0.1 maximum_convert_fusion
  14.8 2.7 fusion.10
  17.5 0.0 copy-start.1
  17.5 0.0 copy-start.3
  17.5 0.0 copy-start.4
  17.5 0.2 copy.26
  17.7 0.9 reshape.101
  18.6 8.6 %all-to-all-start = ((bf16[16,2,2048]{2,1,0:T(2,128)(2,1)}), bf16[16,2,2048]{2,1,0:T(2,128)(2,1)S(1)}, u32[]{:S(2)}, u32[]{:S(2)}) async-start(bf16[16,2,2048]{2,1,0:T(2,128)(2,1)} %reshape.101), calls=%async_computation | async-start | bytes 262144 | tf_op jit(solution)/shard_map/all_to_all | solution.py:45
  27.2 0.0 reduce-scatter.2.cloned.1.call-start
  27.3 0.1 copy.30
  27.3 0.1 fusion.48
  27.4 8.4 %all-to-all-done = bf16[16,2,2048]{2,1,0:T(2,128)(2,1)S(1)} async-done(((bf16[16,2,2048]{2,1,0:T(2,128)(2,1)}), bf16[16,2,2048]{2,1,0:T(2,128)(2,1)S(1)}, u32[]{:S(2)}, u32[]{:S(2)}) %all-to-all-start) | async-done | bytes 131104 | tf_op jit(solution)/shard_map/all_to_all | solution.py:45
  35.8 0.2 reshape.102
  36.1 0.2 convert_reduce_fusion
  36.3 0.0 copy-start.2
  36.3 0.3 copy.27
  36.6 0.2 reshape.91
  36.8 0.3 fusion.8
  37.0 0.0 copy-done.1
  37.0 0.0 copy-done.3
  37.1 0.0 copy-done.4
  37.1 3.3 multiply_reduce_fusion.1
  40.4 0.0 copy-done.2
  40.4 0.4 fusion
  40.7 18.0 %all_to_all.28 = bf16[16,8,2048]{2,1,0:T(8,128)(2,1)S(1)} all-to-all(bf16[16,8,2048]{2,1,0:T(8,128)(2,1)S(1)} %fusion), channel_id=1, replica_groups=mesh['sp'=16,'tp'=16] {'sp'}, dimensions={0} | all-to-all | bytes 1048576 | tf_op jit(solution)/shard_map/all_to_all | solution.py:85
  58.7 1.1 stack.3
  59.8 0.0 copy-start.6
  59.8 187.3 %all_to_all.29 = bf16[16,128,2048]{2,1,0:T(8,128)(2,1)S(1)} all-to-all(bf16[16,128,2048]{2,1,0:T(8,128)(2,1)S(1)} %stack.3), channel_id=1, replica_groups=mesh['sp'=16,'tp'=16] {'tp'}, dimensions={0} | all-to-all | bytes 16777216 | tf_op jit(solution)/shard_map/all_to_all | solution.py:88
  247.0 0.0 copy-done.6
  247.0 0.0 copy-start.7
  247.0 4.0 %fusion.5 = f32[2048,448]{0,1:T(8,128)S(1)} fusion(bf16[2048,2048]{1,0:T(8,128)(2,1)S(1)} %bitcast.99, bf16[1,2048,448]{1,2,0:T(8,128)(2,1)S(1)} %copy-done.6), kind=kOutput, calls=%fused_computation.10 | convolution fusion | flops 3758096384 | bytes 13893632 | tf_op jit(solution)/shard_map/dot_general | solution.py:90
  251.1 0.0 copy-done.7
  251.1 4.3 %multiply_convert_fusion = bf16[2048,448]{0,1:T(8,128)(2,1)S(1)} fusion(f32[2048,448]{0,1:T(8,128)S(1)} %fusion.5, bf16[2048,2048]{1,0:T(8,128)(2,1)S(1)} %bitcast.100, bf16[1,2048,448]{1,2,0:T(8,128)(2,1)S(1)} %copy-done.7), kind=kOutput, calls=%fused_computation.2 | convolution fusion | flops 3763601408 | bytes 15728640 | tf_op jit(solution)/shard_map/dot_general | solution.py:91
  255.4 0.0 copy-done
  255.4 6.9 %convolution_convert_fusion = bf16[2048,2048]{1,0:T(8,128)(2,1)} fusion(bf16[2048,448]{0,1:T(8,128)(2,1)S(1)} %multiply_convert_fusion, bf16[1,448,2048]{2,1,0:T(8,128)(2,1)S(1)} %copy-done), kind=kOutput, calls=%fused_computation.1 | convolution fusion | flops 3762290688 | bytes 12058624 | tf_op jit(solution)/shard_map/dot_general | solution.py:94
  262.3 0.0 copy-start.5
  262.3 0.0 reduce-scatter.2.cloned.1.call-update
  262.3 66.7 %reduce-scatter.2.cloned.1.call-done = bf16[128,2048]{1,0:T(8,128)(2,1)} async-done(((bf16[2048,2048]{1,0:T(8,128)(2,1)}), bf16[128,2048]{1,0:T(8,128)(2,1)}) %reduce-scatter.2.cloned.1.call-update) | async-done | bytes 524304 | tf_op jit(solution)/shard_map/reduce_scatter | solution.py:93
  329.0 7.1 %all-to-all-start.3 = ((bf16[16,8,2048]{2,1,0:T(8,128)(2,1)}), bf16[16,8,2048]{2,1,0:T(8,128)(2,1)S(1)}, u32[]{:S(2)}, u32[]{:S(2)}) async-start(bf16[16,8,2048]{2,1,0:T(8,128)(2,1)} %bitcast.103), calls=%async_computation.4 | async-start | bytes 1048576 | tf_op jit(solution)/shard_map/all_to_all | solution.py:100
  336.1 0.1 mul.497
  336.2 0.0 copy-done.5
  336.2 0.1 copy.31
  336.3 8.5 %all-to-all-done.3 = bf16[16,8,2048]{2,1,0:T(8,128)(2,1)S(1)} async-done(((bf16[16,8,2048]{2,1,0:T(8,128)(2,1)}), bf16[16,8,2048]{2,1,0:T(8,128)(2,1)S(1)}, u32[]{:S(2)}, u32[]{:S(2)}) %all-to-all-start.3) | async-done | bytes 524320 | tf_op jit(solution)/shard_map/all_to_all | solution.py:100
  344.8 1.7 gather_fusion
  346.6 1.7 reshape.92
  348.3 1.5 multiply_reduce_fusion
  349.8 0.8 add_convert_fusion
  (7 shorter events, 0.1 us)
Async XLA Ops:
  6.5 248.9 %copy-start = (bf16[1,448,2048]{2,1,0:T(8,128)(2,1)S(1)}, bf16[1,448,2048]{2,1,0:T(8,128)(2,1)}, u32[]{:S(2)}) copy-start(bf16[1,448,2048]{2,1,0:T(8,128)(2,1)} %param.25) | copy-start | bytes 5505028
  7.8 6.9 %collective-permute-start = (bf16[64,30]{1,0:T(8,128)(2,1)S(1)}, bf16[64,30]{1,0:T(8,128)(2,1)S(1)}, u32[]{:S(2)}, u32[]{:S(2)}) collective-permute-start(bf16[64,30]{1,0:T(8,128)(2,1)S(1)} %slice.254), channel_id=1, source_target_pairs={{0,16},{16,32},{32,48},{48,64},{64,80},{80,96},{96,112},{112,128},... | collective-permute-start | bytes 11528 | tf_op jit(solution)/shard_map/ppermute | solution.py:12
  17.5 19.5 %copy-start.1 = (bf16[64,2048]{1,0:T(8,128)(2,1)S(1)}, bf16[64,2048]{1,0:T(8,128)(2,1)}, u32[]{:S(2)}) copy-start(bf16[64,2048]{1,0:T(8,128)(2,1)} %param.19) | copy-start | bytes 786436
  17.5 19.5 %copy-start.3 = (f32[1024]{0:T(1024)S(1)}, f32[1024]{0:T(1024)}, u32[]{:S(2)}) copy-start(f32[1024]{0:T(1024)} %param.17) | copy-start | bytes 12292
  17.5 19.5 %copy-start.4 = (f32[1024]{0:T(1024)S(1)}, f32[1024]{0:T(1024)}, u32[]{:S(2)}) copy-start(f32[1024]{0:T(1024)} %param.16) | copy-start | bytes 12292
  18.6 17.2 %all-to-all-start = ((bf16[16,2,2048]{2,1,0:T(2,128)(2,1)}), bf16[16,2,2048]{2,1,0:T(2,128)(2,1)S(1)}, u32[]{:S(2)}, u32[]{:S(2)}) async-start(bf16[16,2,2048]{2,1,0:T(2,128)(2,1)} %reshape.101), calls=%async_computation | async-start | bytes 262144 | tf_op jit(solution)/shard_map/all_to_all | solution.py:45
  27.2 301.8 %reduce-scatter.2.cloned.1.call-start = ((), (), s32[]{:S(2)}) async-start(), calls=%async_computation.5 | async-start | bytes 8912896 | tf_op jit(solution)/shard_map/reduce_scatter | solution.py:93
  36.3 4.1 %copy-start.2 = (f32[2048]{0:T(1024)S(1)}, f32[2048]{0:T(1024)}, u32[]{:S(2)}) copy-start(f32[2048]{0:T(1024)} %param.22) | copy-start | bytes 24580
  59.8 187.3 %copy-start.6 = (bf16[1,2048,448]{1,2,0:T(8,128)(2,1)S(1)}, bf16[1,2048,448]{1,2,0:T(8,128)(2,1)}, u32[]{:S(2)}) copy-start(bf16[1,2048,448]{1,2,0:T(8,128)(2,1)} %param.23) | copy-start | bytes 5505028
  247.0 4.0 %copy-start.7 = (bf16[1,2048,448]{1,2,0:T(8,128)(2,1)S(1)}, bf16[1,2048,448]{1,2,0:T(8,128)(2,1)}, u32[]{:S(2)}) copy-start(bf16[1,2048,448]{1,2,0:T(8,128)(2,1)} %param.24) | copy-start | bytes 5505028
  262.3 73.9 %copy-start.5 = (f32[64,2]{0,1:T(2,128)S(1)}, f32[64,2]{0,1:T(2,128)}, u32[]{:S(2)}) copy-start(f32[64,2]{0,1:T(2,128)} %param.21) | copy-start | bytes 1540
  329.0 15.9 %all-to-all-start.3 = ((bf16[16,8,2048]{2,1,0:T(8,128)(2,1)}), bf16[16,8,2048]{2,1,0:T(8,128)(2,1)S(1)}, u32[]{:S(2)}, u32[]{:S(2)}) async-start(bf16[16,8,2048]{2,1,0:T(8,128)(2,1)} %bitcast.103), calls=%async_computation.4 | async-start | bytes 1048576 | tf_op jit(solution)/shard_map/all_to_all | solution.py:100
Sparse Core Ops, SparseCore 0:
  262.4 66.4 reduce-scatter.1
